TPU v7x, 512 devices: a whole 4x4x16 slice. The times are simulated.
512 devices in a mesh: ep: 32 (over z, core), tp: 16 (over y, x).
Axes of the slice: x: 4, y: 4, z: 16, core: 2. Of those that a mesh axis runs over, the one named last changes fastest.
Arguments:
- mix_in: bfloat16 [8192, 2048], P('ep'), may hold values from -6 to 6
- mix_gain: float32 [2048], replicated, may hold values from 0.1 to 1.9
- w_in_x: bfloat16 [2048, 2048], P(None, 'tp'), may hold values from -0.125 to 0.125
- w_in_y: bfloat16 [2048, 2048], P(None, 'tp'), may hold values from -0.125 to 0.125
- conv_taps: float32 [4, 2048], P(None, 'tp'), may hold values from -3 to 3
- recur_gate_w: bfloat16 [16, 128, 128], P('tp'), may hold values from -0.5 to 0.5
- input_gate_w: bfloat16 [16, 128, 128], P('tp'), may hold values from -0.5 to 0.5
- decay_logit: float32 [2048], P('tp'), may hold values from 4 to 20
- decay_shift: float32 [8192, 2048], P('ep', 'tp'), may hold values from -2.2 to 0
- moe_in: bfloat16 [8192, 2048], P('ep'), may hold values from -6 to 6
- moe_gain: float32 [2048], replicated, may hold values from 0.1 to 1.9
- routes: int32 [8192, 2], P('ep'), may hold values from 0 to 31, all different within a row; in each aligned block of 256 rows (0 to 255, 256 to 511, ...) at most 32 rows name the same one
- route_weight: float32 [8192, 2], P('ep'), may hold values from 0.1 to 1
- expert_gate: bfloat16 [32, 2048, 2048], P('ep', None, 'tp'), may hold values from -0.125 to 0.125
- expert_up: bfloat16 [32, 2048, 2048], P('ep', None, 'tp'), may hold values from -0.125 to 0.125
- expert_down: bfloat16 [32, 2048, 2048], P('ep', None, 'tp'), may hold values from -0.125 to 0.125
Outputs:
- mixer_out: bfloat16 [8192, 2048], P('ep', 'tp')
- moe_out: bfloat16 [8192, 2048], P('ep', 'tp')
Inputs may be any that keep to these rules, and one draw needn't show every extreme that they name: `routes`: each row names 2 different experts. Among the rows of one index of ep no expert is named more than 32 times, a bound that some block reaches.
All inputs are finite; a program needn't handle non-finite values.
Results may differ from a plain program's by a relative error of at most 0.0095.
Values may be sent and summed in bfloat16 or wider, within the bound.
A program may use at most 64 MiB of HBM per device.

v0:
```python
import jax
import jax.numpy as jnp
from jax import lax
from jax.sharding import PartitionSpec as P

epsilon = 1e-06
lru_scale = 8.0


def from_behind(value, axis, by):
    count = lax.axis_size(axis)
    pairs = [(i, i + by) for i in range(count) if 0 <= i + by < count]
    return lax.ppermute(value, axis, pairs)


def copy_for_each(value, axis):
    count = lax.axis_size(axis)
    return lax.all_to_all(
        jnp.broadcast_to(value[None], (count, *value.shape)), axis, 0, 0, tiled=True
    )


def all_in_one(value, axis):
    leaves = jax.tree.leaves(value)
    sequence = sorted(range(len(leaves)), key=lambda k: -leaves[k].size)
    width = (1, *leaves[sequence[0]].shape)[-1]
    lines = [
        jnp.pad(leaves[k].reshape(-1), (0, -leaves[k].size % width)).reshape(-1, width)
        for k in sequence
    ]
    both, at, found = (copy_for_each(jnp.concatenate(lines), axis), 0, {})
    for k, line in zip(sequence, lines):
        slab = both[:, at : at + len(line)].reshape(len(both), -1)
        found[k] = slab[:, : leaves[k].size].reshape(-1, *leaves[k].shape)
        at += len(line)
    numbers = iter(range(len(leaves)))
    return jax.tree.map(lambda _: found[next(numbers)], value)


def combined_pairwise(pieces, combine):
    while len(jax.tree.leaves(pieces)[0]) > 1:
        pieces = jax.vmap(combine)(
            *(jax.tree.map(lambda part: part[side::2], pieces) for side in (0, 1))
        )
    return jax.tree.map(lambda part: part[0], pieces)


def entering(value, axis, combine, identity):
    count, index = (lax.axis_size(axis), lax.axis_index(axis))
    passed = jnp.arange(count) < index

    def kept(part, zero, own):
        part = jnp.where(
            passed.reshape(-1, *(1 for _ in own.shape)), part, jnp.asarray(zero, own.dtype)
        )
        return part

    pieces = all_in_one(value, axis)
    return combined_pairwise(jax.tree.map(kept, pieces, identity, value), combine)


def norm_rows(rows, gain):
    widened = rows.astype(jnp.float32)
    scaled = widened * lax.rsqrt(jnp.mean(widened * widened, axis=-1, keepdims=True) + epsilon)
    return (scaled * gain[None, :]).astype(jnp.bfloat16)


def link(earlier, later):
    return (earlier[0] * later[0], later[0] * earlier[1] + later[1])


def local(
    mix_in,
    mix_gain,
    w_in_x,
    w_in_y,
    conv_taps,
    recur_gate_w,
    input_gate_w,
    decay_logit,
    decay_shift,
    moe_in,
    moe_gain,
    routes,
    route_weight,
    expert_gate,
    expert_up,
    expert_down,
):
    row_count = mix_in.shape[0]
    width_dev = w_in_x.shape[1]
    heads_dev = recur_gate_w.shape[0]
    block_size = recur_gate_w.shape[1]
    tap_count = conv_taps.shape[0]
    mixer_rows = norm_rows(mix_in, mix_gain)
    x_branch = jnp.dot(mixer_rows, w_in_x, preferred_element_type=jnp.float32).astype(jnp.bfloat16)
    y_branch = jnp.dot(mixer_rows, w_in_y, preferred_element_type=jnp.float32).astype(jnp.bfloat16)
    previous = from_behind(x_branch[row_count - (tap_count - 1) :], "ep", 1)
    padded = jnp.concatenate([previous, x_branch], axis=0)
    conv_sum = jnp.zeros((row_count, width_dev), jnp.float32)
    for tap_index in range(tap_count):
        conv_sum = conv_sum + conv_taps[tap_index][None, :] * padded[
            tap_index : tap_index + row_count
        ].astype(jnp.float32)
    x_conv = conv_sum.astype(jnp.bfloat16)
    heads_in = x_conv.reshape(row_count, heads_dev, block_size)
    gate_a = jnp.einsum(
        "thi,hij->thj", heads_in, recur_gate_w, preferred_element_type=jnp.float32
    ).reshape(row_count, width_dev)
    gate_x = jnp.einsum(
        "thi,hij->thj", heads_in, input_gate_w, preferred_element_type=jnp.float32
    ).reshape(row_count, width_dev)
    log_decay = (
        -lru_scale * jax.nn.sigmoid(gate_a) * jax.nn.softplus(-decay_logit)[None, :] + decay_shift
    )
    lru_drive = (
        jnp.sqrt(-jnp.expm1(2.0 * log_decay)) * jax.nn.sigmoid(gate_x) * x_conv.astype(jnp.float32)
    )
    through, local_state = lax.associative_scan(link, (jnp.exp(log_decay), lru_drive), axis=0)
    identity = (jnp.ones((width_dev,), jnp.float32), jnp.zeros((width_dev,), jnp.float32))
    carried = entering((through[row_count - 1], local_state[row_count - 1]), "ep", link, identity)
    lru_state = local_state + through * carried[1][None, :]
    mixer_out = (lru_state * jax.nn.gelu(y_branch.astype(jnp.float32))).astype(jnp.bfloat16)
    moe_rows = norm_rows(moe_in, moe_gain)
    token_count = moe_rows.shape[0]
    feature_count = moe_rows.shape[1]
    choose_count = routes.shape[1]
    expert_count = lax.axis_size("ep")
    capacity = 2 * token_count * choose_count // expert_count
    slot_total = expert_count * capacity
    expert_ids = routes.reshape(-1)
    onehot = (expert_ids[:, None] == jnp.arange(expert_count, dtype=jnp.int32)[None, :]).astype(
        jnp.int32
    )
    slot_rank = jnp.sum(jnp.cumsum(onehot, axis=0) * onehot, axis=1) - 1
    slot_index = expert_ids * capacity + slot_rank
    token_index = jnp.repeat(jnp.arange(token_count, dtype=jnp.int32), choose_count)
    slot_owner = jnp.full((slot_total,), token_count, jnp.int32).at[slot_index].set(token_index)
    padded_rows = jnp.concatenate([moe_rows, jnp.zeros((1, feature_count), jnp.bfloat16)], axis=0)
    outgoing = padded_rows[slot_owner].reshape(expert_count, capacity, feature_count)
    column_width = feature_count // lax.axis_size("tp")
    own_columns = lax.dynamic_slice_in_dim(
        outgoing, lax.axis_index("tp") * column_width, column_width, 2
    )
    incoming = lax.all_to_all(own_columns, "ep", split_axis=0, concat_axis=0, tiled=True)
    piece = lax.all_gather(incoming, "tp", axis=2, tiled=True)
    flat_rows = piece.reshape(slot_total, piece.shape[2])
    gate_rows = expert_gate[0]
    up_rows = expert_up[0]
    gate_proj = jnp.dot(flat_rows, gate_rows, preferred_element_type=jnp.float32)
    up_proj = jnp.dot(flat_rows, up_rows, preferred_element_type=jnp.float32)
    hidden = (jax.nn.silu(gate_proj) * up_proj).astype(jnp.bfloat16)
    down_rows = expert_down[0]
    columns = jnp.dot(
        lax.all_gather(hidden, "tp", axis=1, tiled=True),
        down_rows,
        preferred_element_type=jnp.float32,
    )
    results = columns.astype(jnp.bfloat16).reshape(expert_count, capacity, expert_down.shape[2])
    returned = lax.all_to_all(results, "ep", split_axis=0, concat_axis=0, tiled=True).reshape(
        slot_total, expert_down.shape[2]
    )
    picked = (
        returned[slot_index]
        .astype(jnp.float32)
        .reshape(token_count, choose_count, expert_down.shape[2])
    )
    route_share = route_weight / jnp.sum(route_weight, axis=1, keepdims=True)
    moe_out = jnp.sum(route_share[:, :, None] * picked, axis=1).astype(jnp.bfloat16)
    return (mixer_out, moe_out)


def solution(mesh):
    placed = (
        P("ep", None),
        P(),
        P(None, "tp"),
        P(None, "tp"),
        P(None, "tp"),
        P("tp", None, None),
        P("tp", None, None),
        P("tp"),
        P("ep", "tp"),
        P("ep", None),
        P(),
        P("ep", None),
        P("ep", None),
        P("ep", None, "tp"),
        P("ep", None, "tp"),
        P("ep", None, "tp"),
    )
    return jax.shard_map(
        local, mesh=mesh, in_specs=placed, out_specs=(P("ep", "tp"), P("ep", "tp")), check_vma=False
    )
```

profile of v0, /device:TPU:1, one launch (start us, length us, event | category | flops | bytes accessed | tf_op | source)
XLA Modules:
  0.0 251.2 jit_solution(5826928221437767677)
XLA Ops:
  7.2 0.0 copy-start
  7.2 0.0 copy-start.2
  7.2 0.0 all-gather.3.cloned.1.call-start
  7.3 0.9 copy.27
  8.2 0.1 eq.29
  8.3 0.1 eq.25
  8.5 0.7 broadcast_multiply_fusion
  9.2 1.2 reduce-window.6
  10.3 0.2 slice_reduce_fusion
  10.6 0.1 fusion.43
  10.7 0.1 copy.26
  10.9 0.1 mul.375
  11.0 0.1 reshape.156
  11.2 2.4 scatter_custom_fusion
  13.6 1.5 fusion.3
  15.2 0.3 fusion.5
  15.5 0.1 concatenate.67
  15.6 0.0 copy-start.3
  15.6 6.0 %gather_fusion = bf16[1024,2048]{1,0:T(8,128)(2,1)} fusion(bf16[257,2048]{1,0:T(8,128)(2,1)S(1)} %concatenate.67, s32[1024]{0:T(1024)S(1)} %fusion.51), kind=kCustom, calls=%fused_computation | custom fusion | bytes 8392704 | tf_op jit(solution)/shard_map/gather | solution.py:140
  21.6 1.0 constant_dynamic-slice_fusion
  22.6 0.0 copy-start.5
  22.6 38.9 %all_to_all.15 = bf16[32,32,128]{2,1,0:T(8,128)(2,1)} all-to-all(bf16[32,32,128]{2,1,0:T(8,128)(2,1)S(1)} %constant_dynamic-slice_fusion), channel_id=1, replica_groups=mesh['ep'=32,'tp'=16] {'ep'}, dimensions={0} | all-to-all | bytes 524288 | tf_op jit(solution)/shard_map/all_to_all | solution.py:145
  61.5 0.0 all-gather.3.cloned.1.call-update
  61.5 0.0 all-gather.5.cloned.1.call-start
  61.6 0.3 fusion
  61.9 0.5 convolution_convert_fusion.2
  62.4 2.2 collective-permute-start
  64.7 59.1 %all-gather.3.cloned.1.call-done = bf16[32,32,2048]{2,1,0:T(8,128)(2,1)} async-done(((bf16[32,32,128]{2,1,0:T(8,128)(2,1)}), bf16[32,32,2048]{2,1,0:T(8,128)(2,1)}) %all-gather.3.cloned.1.call-update) | async-done | bytes 4194320 | tf_op jit(solution)/shard_map/all_gather | solution.py:146
  123.8 3.6 %fusion.20 = f32[1024,128]{1,0:T(8,128)S(1)} fusion(bf16[1024,2048]{1,0:T(8,128)(2,1)} %bitcast.61, bf16[1,2048,128]{2,1,0:T(8,128)(2,1)S(1)} %copy-done), kind=kOutput, calls=%fused_computation.33 | convolution fusion | flops 536870912 | bytes 5242880 | tf_op jit(solution)/shard_map/dot_general | solution.py:150
  127.4 0.0 copy-start.15
  127.4 0.0 copy-start.11
  127.4 2.0 fusion.6
  129.4 0.0 all-gather.5.cloned.1.call-update
  129.5 0.1 add_convert_fusion
  129.6 0.2 fusion.61
  129.8 0.2 fusion.16
  132.0 0.6 broadcast_in_dim.27
  132.6 14.4 %all-to-all-start = ((f32[32,2,128]{2,1,0:T(2,128)}), f32[32,2,128]{2,1,0:T(2,128)S(1)}, u32[]{:S(2)}, u32[]{:S(2)}) async-start(f32[32,2,128]{2,1,0:T(2,128)} %broadcast_in_dim.27), calls=%async_computation | async-start | bytes 65536 | tf_op jit(solution)/shard_map/all_to_all | solution.py:18
  147.0 0.1 copy.25
  147.2 11.9 %all-to-all-done = f32[32,2,128]{2,1,0:T(2,128)S(1)} async-done(((f32[32,2,128]{2,1,0:T(2,128)}), f32[32,2,128]{2,1,0:T(2,128)S(1)}, u32[]{:S(2)}, u32[]{:S(2)}) %all-to-all-start) | async-done | bytes 32800 | tf_op jit(solution)/shard_map/all_to_all | solution.py:18
  159.1 0.1 broadcast_select_fusion.1
  159.3 41.9 %all-gather.5.cloned.1.call-done = bf16[1024,2048]{1,0:T(8,128)(2,1)} async-done(((bf16[1024,128]{1,0:T(8,128)(2,1)}), bf16[1024,2048]{1,0:T(8,128)(2,1)}) %all-gather.5.cloned.1.call-update) | async-done | bytes 4194320 | tf_op jit(solution)/shard_map/all_gather | solution.py:155
  201.2 4.1 %convolution_convert_fusion = bf16[1024,128]{1,0:T(8,128)(2,1)} fusion(bf16[1024,2048]{1,0:T(8,128)(2,1)} %all-gather.5.cloned.1.call-done, bf16[1,2048,128]{2,1,0:T(8,128)(2,1)S(1)} %copy-done.9), kind=kOutput, calls=%fused_computation.15 | convolution fusion | flops 537001984 | bytes 4980736 | tf_op jit(solution)/shard_map/dot_general | solution.py:154
  205.3 14.4 %all-to-all-start.2 = ((bf16[32,32,128]{2,1,0:T(8,128)(2,1)}), bf16[32,32,128]{2,1,0:T(8,128)(2,1)S(1)}, u32[]{:S(2)}, u32[]{:S(2)}) async-start(bf16[32,32,128]{2,1,0:T(8,128)(2,1)} %bitcast.17), calls=%async_computation.2 | async-start | bytes 524288 | tf_op jit(solution)/shard_map/all_to_all | solution.py:160
  220.0 1.1 fusion.37
  221.1 20.9 %all-to-all-done.2 = bf16[32,32,128]{2,1,0:T(8,128)(2,1)S(1)} async-done(((bf16[32,32,128]{2,1,0:T(8,128)(2,1)}), bf16[32,32,128]{2,1,0:T(8,128)(2,1)S(1)}, u32[]{:S(2)}, u32[]{:S(2)}) %all-to-all-start.2) | async-done | bytes 262176 | tf_op jit(solution)/shard_map/all_to_all | solution.py:160
  242.0 1.3 gather_fusion.1
  243.3 1.1 fusion.24
  (190 shorter events, 1.8 us)
Async XLA Ops:
  7.2 116.6 %copy-start = (bf16[1,2048,128]{2,1,0:T(8,128)(2,1)S(1)}, bf16[1,2048,128]{2,1,0:T(8,128)(2,1)}, u32[]{:S(2)}) copy-start(bf16[1,2048,128]{2,1,0:T(8,128)(2,1)} %param.29) | copy-start | bytes 1572868
  7.2 8.0 %copy-start.2 = (bf16[256,2048]{1,0:T(8,128)(2,1)S(1)}, bf16[256,2048]{1,0:T(8,128)(2,1)}, u32[]{:S(2)}) copy-start(bf16[256,2048]{1,0:T(8,128)(2,1)} %param.25) | copy-start | bytes 3145732
  7.2 8.0 %copy-start.4 = (f32[2048]{0:T(1024)S(1)}, f32[2048]{0:T(1024)}, u32[]{:S(2)}) copy-start(f32[2048]{0:T(1024)} %param.26) | copy-start | bytes 24580
  7.2 116.6 %all-gather.3.cloned.1.call-start = ((), (), s32[]{:S(2)}) async-start(), calls=%async_computation.3 | async-start | bytes 4456448 | tf_op jit(solution)/shard_map/all_gather | solution.py:146
  15.6 46.0 %copy-start.3 = (bf16[256,2048]{1,0:T(8,128)(2,1)S(1)}, bf16[256,2048]{1,0:T(8,128)(2,1)}, u32[]{:S(2)}) copy-start(bf16[256,2048]{1,0:T(8,128)(2,1)} %param.16) | copy-start | bytes 3145732
  21.6 40.3 %copy-start.7 = (bf16[2048,128]{1,0:T(8,128)(2,1)S(1)}, bf16[2048,128]{1,0:T(8,128)(2,1)}, u32[]{:S(2)}) copy-start(bf16[2048,128]{1,0:T(8,128)(2,1)} %param.18) | copy-start | bytes 1572868
  21.6 40.3 %copy-start.14 = (f32[2048]{0:T(1024)S(1)}, f32[2048]{0:T(1024)}, u32[]{:S(2)}) copy-start(f32[2048]{0:T(1024)} %param.17) | copy-start | bytes 24580
  22.6 42.1 %copy-start.5 = (f32[256,2]{0,1:T(2,128)S(1)}, f32[256,2]{0,1:T(2,128)}, u32[]{:S(2)}) copy-start(f32[256,2]{0,1:T(2,128)} %param.28) | copy-start | bytes 6148
  61.5 139.6 %all-gather.5.cloned.1.call-start = ((), (), s32[]{:S(2)}) async-start(), calls=%async_computation.4 | async-start | bytes 4456448 | tf_op jit(solution)/shard_map/all_gather | solution.py:155
  62.4 67.1 %collective-permute-start = (bf16[3,128]{1,0:T(4,128)(2,1)S(1)}, bf16[3,128]{1,0:T(4,128)(2,1)S(1)}, u32[]{:S(2)}, u32[]{:S(2)}) collective-permute-start(bf16[3,128]{1,0:T(4,128)(2,1)S(1)} %slice.443), channel_id=1, source_target_pairs={{0,16},{16,32},{32,48},{48,64},{64,80},{80,96},{96,112},{112,128},... | collective-permute-start | bytes 2312 | tf_op jit(solution)/shard_map/ppermute | solution.py:13
  123.8 3.6 %copy-start.1 = (bf16[32,32,2048]{2,1,0:T(8,128)(2,1)S(1)}, bf16[32,32,2048]{2,1,0:T(8,128)(2,1)}, u32[]{:S(2)}) copy-start(bf16[32,32,2048]{2,1,0:T(8,128)(2,1)} %all-gather.3.cloned.1.call-done) | copy-start | bytes 12582916
  123.8 3.6 %copy-start.8 = (bf16[1,2048,128]{2,1,0:T(8,128)(2,1)S(1)}, bf16[1,2048,128]{2,1,0:T(8,128)(2,1)}, u32[]{:S(2)}) copy-start(bf16[1,2048,128]{2,1,0:T(8,128)(2,1)} %param.30) | copy-start | bytes 1572868
  127.4 2.1 copy-start.6
  127.4 2.1 copy-start.15
  127.4 2.2 copy-start.11
  127.4 2.2 copy-start.12
  127.4 2.4 copy-start.13
  131.3 69.8 %copy-start.9 = (bf16[1,2048,128]{2,1,0:T(8,128)(2,1)S(1)}, bf16[1,2048,128]{2,1,0:T(8,128)(2,1)}, u32[]{:S(2)}) copy-start(bf16[1,2048,128]{2,1,0:T(8,128)(2,1)} %param.31) | copy-start | bytes 1572868
  132.6 26.4 %all-to-all-start = ((f32[32,2,128]{2,1,0:T(2,128)}), f32[32,2,128]{2,1,0:T(2,128)S(1)}, u32[]{:S(2)}, u32[]{:S(2)}) async-start(f32[32,2,128]{2,1,0:T(2,128)} %broadcast_in_dim.27), calls=%async_computation | async-start | bytes 65536 | tf_op jit(solution)/shard_map/all_to_all | solution.py:18
  159.3 60.7 %copy-start.10 = (bf16[2048,128]{1,0:T(8,128)(2,1)S(1)}, bf16[2048,128]{1,0:T(8,128)(2,1)}, u32[]{:S(2)}) copy-start(bf16[2048,128]{1,0:T(8,128)(2,1)} %param.19) | copy-start | bytes 1572868
  205.3 36.6 %all-to-all-start.2 = ((bf16[32,32,128]{2,1,0:T(8,128)(2,1)}), bf16[32,32,128]{2,1,0:T(8,128)(2,1)S(1)}, u32[]{:S(2)}, u32[]{:S(2)}) async-start(bf16[32,32,128]{2,1,0:T(8,128)(2,1)} %bitcast.17), calls=%async_computation.2 | async-start | bytes 524288 | tf_op jit(solution)/shard_map/all_to_all | solution.py:160
Sparse Core Ops, SparseCore 0:
  61.7 62.0 all-gather.2
  129.6 71.5 all-gather.4
where the time goes:
time: 252 us; the launch traced here: 251 us
  waiting for transfers between devices  134 us (53%)
  blocking collectives  38.9 us (15%)
  starting transfers between devices  31.1 us (12%)
  between operations  15.2 us (6%)
  local copies, waits for them, and re-layouts  14.7 us (6%)
  matrix products  11.7 us (5%)
  other arithmetic  5.83 us (2%)
    all_gather x1, waiting for transfers between devices, local(): piece = lax.all_gather(incoming, 'tp', axis=2, tiled=True)  59.1 us
    all_gather x1, waiting for transfers between devices, local(): lax.all_gather(hidden, 'tp', axis=1, tiled=True)  41.9 us
    all_to_all x1, blocking collectives, local(): lax.all_to_all(own_columns, 'ep', split_axis=0, concat_axis=0, tiled=True)  38.9 us
    all_to_all x1, waiting for transfers between devices, local(): lax.all_to_all(results, 'ep', split_axis=0, concat_axis=0, tiled=True)  20.9 us
    all_to_all x1, starting transfers between devices, copy_for_each(): lax.all_to_all(jnp.broadcast_to(value[None], (count, *value.shape)), axis...  14.4 us
    all_to_all x1, starting transfers between devices, local(): lax.all_to_all(results, 'ep', split_axis=0, concat_axis=0, tiled=True)  14.4 us
    all_to_all x1, waiting for transfers between devices, copy_for_each(): lax.all_to_all(jnp.broadcast_to(value[None], (count, *value.shape)), axis...  11.9 us
    gather x1, local copies, waits for them, and re-layouts, local(): padded_rows[slot_owner].reshape(expert_count, capacity, feature_count)  5.97 us
  transfers between devices with their start and end apart: 5, of which 4 were waited for; matrix products, arithmetic and copies ran while one was open for 4% of the time, Pallas kernels for 0%

commit v1 on v0

--- a/solution.py
+++ b/solution.py
@@ -1,10 +1,39 @@
+import functools
 import jax
 import jax.numpy as jnp
 from jax import lax
 from jax.sharding import PartitionSpec as P
+from jax.lax import axis_index, axis_size, ppermute
 
 epsilon = 1e-06
 lru_scale = 8.0
+
+
+def tell_classes(arr_in, chip_axis, d_out):
+    r1, carry_out, side_arr = (axis_size(chip_axis), axis_index(chip_axis), arr_in.shape[d_out])
+    res = lax.dynamic_update_slice_in_dim(
+        jnp.zeros(
+            tuple((j * r1 if q == d_out else j for q, j in enumerate(arr_in.shape))), arr_in.dtype
+        ),
+        arr_in,
+        carry_out * side_arr,
+        axis=d_out,
+    )
+    parts_out = left_arr = arr_in
+    for dev_i in [*range(1, r1 // 2 + 1)]:
+        parts_out = ppermute(parts_out, chip_axis, tuple(((q, (q + 1) % r1) for q in range(r1))))
+        res = lax.dynamic_update_slice_in_dim(
+            res, parts_out, (carry_out - dev_i) % r1 * side_arr, axis=d_out
+        )
+        if 2 * dev_i < r1:
+            left_arr = ppermute(left_arr, chip_axis, tuple(((q, (q - 1) % r1) for q in range(r1))))
+            res = lax.dynamic_update_slice_in_dim(
+                res, left_arr, (carry_out + dev_i) % r1 * side_arr, axis=d_out
+            )
+    return res
+
+
+pack_notes_in = functools.partial(tell_classes, chip_axis="tp", d_out=1)
 
 
 def from_behind(value, axis, by):
@@ -151,11 +180,7 @@
     up_proj = jnp.dot(flat_rows, up_rows, preferred_element_type=jnp.float32)
     hidden = (jax.nn.silu(gate_proj) * up_proj).astype(jnp.bfloat16)
     down_rows = expert_down[0]
-    columns = jnp.dot(
-        lax.all_gather(hidden, "tp", axis=1, tiled=True),
-        down_rows,
-        preferred_element_type=jnp.float32,
-    )
+    columns = jnp.dot(pack_notes_in(hidden), down_rows, preferred_element_type=jnp.float32)
     results = columns.astype(jnp.bfloat16).reshape(expert_count, capacity, expert_down.shape[2])
     returned = lax.all_to_all(results, "ep", split_axis=0, concat_axis=0, tiled=True).reshape(
         slot_total, expert_down.shape[2]

time: 252 us -> 293 us (1.16)
  starting transfers between devices: 31.1 us -> 98.9 us
  waiting for transfers between devices: 134 us -> 88.2 us
  local copies, waits for them, and re-layouts: 14.7 us -> 30.2 us
    ppermute x0 -> x15, starting transfers between devices: none -> 64.3 us  [the longest x7 47.9 us: tell_classes(): ppermute(left_arr, chip_axis, tuple(((q, (q - 1) % r1) for q in range(r1))))]
    all_gather x1 -> x0, waiting for transfers between devices: 41.9 us -> none  [local(): lax.all_gather(hidden, 'tp', axis=1, tiled=True)]
    dynamic_update_slice x0 -> x15, local copies, waits for them, and re-layouts: none -> 12.3 us  [the longest x8 7.02 us: tell_classes(): lax.dynamic_update_slice_in_dim(res, parts_out, (carry_out - dev_i) % r1...]
    ppermute x0 -> x15, waiting for transfers between devices: none -> 10.2 us  [the longest x8 7.76 us: tell_classes(): ppermute(parts_out, chip_axis, tuple(((q, (q + 1) % r1) for q in range(r1...]
    all_to_all x1, waiting for transfers between devices: 11.9 us -> 2.64 us  [copy_for_each(): lax.all_to_all(jnp.broadcast_to(value[None], (count, *value.shape)), axis...]
    all_gather x1, waiting for transfers between devices: 59.1 us -> 54.8 us  [local(): piece = lax.all_gather(incoming, 'tp', axis=2, tiled=True)]
  transfers between devices with their start and end apart: 5 -> 19, of which waited for: 4 -> 8; matrix products, arithmetic and copies ran while one was open for 4% -> 6% of each run, Pallas kernels for 0% -> 0%
where the time goes in v1:
time: 293 us; the launch traced here: 292 us
  starting transfers between devices  98.9 us (34%)
  waiting for transfers between devices  88.2 us (30%)
  blocking collectives  38.9 us (13%)
  local copies, waits for them, and re-layouts  30.2 us (10%)
  between operations  15.7 us (5%)
  matrix products  13.2 us (5%)
  other arithmetic  7.05 us (2%)
    all_gather x1, waiting for transfers between devices, local(): piece = lax.all_gather(incoming, 'tp', axis=2, tiled=True)  54.8 us
    ppermute x7, starting transfers between devices, tell_classes(): ppermute(left_arr, chip_axis, tuple(((q, (q - 1) % r1) for q in range(r1))))  47.9 us
    all_to_all x1, blocking collectives, local(): lax.all_to_all(own_columns, 'ep', split_axis=0, concat_axis=0, tiled=True)  38.9 us
    all_to_all x1, waiting for transfers between devices, local(): lax.all_to_all(results, 'ep', split_axis=0, concat_axis=0, tiled=True)  19.8 us
    all_to_all x1, starting transfers between devices, local(): lax.all_to_all(results, 'ep', split_axis=0, concat_axis=0, tiled=True)  16.9 us
    ppermute x8, starting transfers between devices, tell_classes(): ppermute(parts_out, chip_axis, tuple(((q, (q + 1) % r1) for q in range(r1...  16.4 us
    all_to_all x1, starting transfers between devices, copy_for_each(): lax.all_to_all(jnp.broadcast_to(value[None], (count, *value.shape)), axis...  15.3 us
    ppermute x8, waiting for transfers between devices, tell_classes(): ppermute(parts_out, chip_axis, tuple(((q, (q + 1) % r1) for q in range(r1...  7.76 us
  transfers between devices with their start and end apart: 19, of which 8 were waited for; matrix products, arithmetic and copies ran while one was open for 6% of the time, Pallas kernels for 0%

profile of v1, /device:TPU:1, one launch (start us, length us, event | category | flops | bytes accessed | tf_op | source)
XLA Modules:
  0.0 292.1 jit_solution(8643809773301820393)
XLA Ops:
  7.2 0.9 copy.27
  9.1 1.2 reduce-window.6
  11.1 2.4 scatter_custom_fusion
  13.6 1.5 fusion.3
  15.1 1.5 fusion.5
  16.7 6.0 %gather_fusion = bf16[1024,2048]{1,0:T(8,128)(2,1)} fusion(bf16[257,2048]{1,0:T(8,128)(2,1)S(1)} %concatenate.67, s32[1024]{0:T(1024)S(1)} %fusion.51), kind=kCustom, calls=%fused_computation | custom fusion | bytes 8392704 | tf_op jit(solution)/shard_map/gather | solution.py:169
  22.8 1.1 constant_dynamic-slice_fusion
  23.9 38.9 %all_to_all.15 = bf16[32,32,128]{2,1,0:T(8,128)(2,1)} all-to-all(bf16[32,32,128]{2,1,0:T(8,128)(2,1)S(1)} %constant_dynamic-slice_fusion), channel_id=1, replica_groups=mesh['ep'=32,'tp'=16] {'ep'}, dimensions={0} | all-to-all | bytes 524288 | tf_op jit(solution)/shard_map/all_to_all | solution.py:174
  63.1 1.5 convolution_convert_fusion.2
  64.7 2.4 collective-permute-start
  70.2 54.8 %all-gather.2.cloned.1.call-done = bf16[32,32,2048]{2,1,0:T(8,128)(2,1)} async-done(((bf16[32,32,128]{2,1,0:T(8,128)(2,1)}), bf16[32,32,2048]{2,1,0:T(8,128)(2,1)}) %all-gather.2.cloned.1.call-update) | async-done | bytes 4194320 | tf_op jit(solution)/shard_map/all_gather | solution.py:175
  125.0 3.6 %fusion.20 = f32[1024,128]{1,0:T(8,128)S(1)} fusion(bf16[1024,2048]{1,0:T(8,128)(2,1)} %bitcast.63, bf16[1,2048,128]{2,1,0:T(8,128)(2,1)S(1)} %copy-done.4), kind=kOutput, calls=%fused_computation.33 | convolution fusion | flops 536870912 | bytes 5242880 | tf_op jit(solution)/shard_map/dot_general | solution.py:179
  129.2 1.4 constant_dynamic-update-slice_fusion.15
  130.5 2.0 copy-done.2
  132.5 2.8 collective-permute-start.1
  136.1 5.8 %collective-permute-start.2 = (bf16[1024,128]{1,0:T(8,128)(2,1)S(1)}, bf16[1024,128]{1,0:T(8,128)(2,1)S(1)}, u32[]{:S(2)}, u32[]{:S(2)}) collective-permute-start(bf16[1024,128]{1,0:T(8,128)(2,1)S(1)} %get-tuple-element.55), channel_id=1, source_target_pairs={{0,15},{1,0},{2,1},{3,2},{4,3},{5,4},{6,5},{7,6},{8,7},{9,8},{10,9... | collective-permute-start | bytes 786440 | tf_op jit(solution)/shard_map/ppermute | solution.py:29
  141.9 1.7 collective-permute-done.1
  143.5 1.9 collective-permute-start.3
  146.1 15.3 %all-to-all-start = ((f32[32,2,128]{2,1,0:T(2,128)}), f32[32,2,128]{2,1,0:T(2,128)S(1)}, u32[]{:S(2)}, u32[]{:S(2)}) async-start(f32[32,2,128]{2,1,0:T(2,128)} %broadcast_in_dim.50), calls=%async_computation | async-start | bytes 65536 | tf_op jit(solution)/shard_map/all_to_all | solution.py:47
  161.9 7.0 %collective-permute-start.4 = (bf16[1024,128]{1,0:T(8,128)(2,1)S(1)}, bf16[1024,128]{1,0:T(8,128)(2,1)S(1)}, u32[]{:S(2)}, u32[]{:S(2)}) collective-permute-start(bf16[1024,128]{1,0:T(8,128)(2,1)S(1)} %collective-permute-done.2), channel_id=1, source_target_pairs={{0,15},{1,0},{2,1},{3,2},{4,3},{5,4},{6,5},{7,6},{8,7},{9,8},{10,9... | collective-permute-start | bytes 786440 | tf_op jit(solution)/shard_map/ppermute | solution.py:29
  168.9 1.9 collective-permute-start.5
  170.8 2.6 all-to-all-done
  174.3 7.4 %collective-permute-start.6 = (bf16[1024,128]{1,0:T(8,128)(2,1)S(1)}, bf16[1024,128]{1,0:T(8,128)(2,1)S(1)}, u32[]{:S(2)}, u32[]{:S(2)}) collective-permute-start(bf16[1024,128]{1,0:T(8,128)(2,1)S(1)} %collective-permute-done.4), channel_id=1, source_target_pairs={{0,15},{1,0},{2,1},{3,2},{4,3},{5,4},{6,5},{7,6},{8,7},{9,8},{10,9... | collective-permute-start | bytes 786440 | tf_op jit(solution)/shard_map/ppermute | solution.py:29
  181.7 1.9 collective-permute-start.7
  183.7 0.8 constant_dynamic-update-slice_fusion.14
  184.5 1.7 collective-permute-done.6
  186.2 7.4 %collective-permute-start.8 = (bf16[1024,128]{1,0:T(8,128)(2,1)S(1)}, bf16[1024,128]{1,0:T(8,128)(2,1)S(1)}, u32[]{:S(2)}, u32[]{:S(2)}) collective-permute-start(bf16[1024,128]{1,0:T(8,128)(2,1)S(1)} %collective-permute-done.6), channel_id=1, source_target_pairs={{0,15},{1,0},{2,1},{3,2},{4,3},{5,4},{6,5},{7,6},{8,7},{9,8},{10,9... | collective-permute-start | bytes 786440 | tf_op jit(solution)/shard_map/ppermute | solution.py:29
  194.4 1.9 collective-permute-start.9
  196.3 0.8 constant_dynamic-update-slice_fusion.12
  197.1 0.8 constant_dynamic-update-slice_fusion.11
  197.9 6.9 %collective-permute-start.10 = (bf16[1024,128]{1,0:T(8,128)(2,1)S(1)}, bf16[1024,128]{1,0:T(8,128)(2,1)S(1)}, u32[]{:S(2)}, u32[]{:S(2)}) collective-permute-start(bf16[1024,128]{1,0:T(8,128)(2,1)S(1)} %collective-permute-done.8), channel_id=1, source_target_pairs={{0,15},{1,0},{2,1},{3,2},{4,3},{5,4},{6,5},{7,6},{8,7},{9,8},{10,9... | collective-permute-start | bytes 786440 | tf_op jit(solution)/shard_map/ppermute | solution.py:29
  204.8 0.8 constant_dynamic-update-slice_fusion.10
  205.6 1.9 collective-permute-start.11
  208.2 1.7 constant_dynamic-update-slice_fusion.8
  209.9 6.7 %collective-permute-start.12 = (bf16[1024,128]{1,0:T(8,128)(2,1)S(1)}, bf16[1024,128]{1,0:T(8,128)(2,1)S(1)}, u32[]{:S(2)}, u32[]{:S(2)}) collective-permute-start(bf16[1024,128]{1,0:T(8,128)(2,1)S(1)} %collective-permute-done.10), channel_id=1, source_target_pairs={{0,15},{1,0},{2,1},{3,2},{4,3},{5,4},{6,5},{7,6},{8,7},{9,8},{10,9... | collective-permute-start | bytes 786440 | tf_op jit(solution)/shard_map/ppermute | solution.py:29
  216.6 0.8 constant_dynamic-update-slice_fusion.7
  217.4 1.9 collective-permute-start.13
  220.8 6.7 %collective-permute-start.14 = (bf16[1024,128]{1,0:T(8,128)(2,1)S(1)}, bf16[1024,128]{1,0:T(8,128)(2,1)S(1)}, u32[]{:S(2)}, u32[]{:S(2)}) collective-permute-start(bf16[1024,128]{1,0:T(8,128)(2,1)S(1)} %collective-permute-done.12), channel_id=1, source_target_pairs={{0,15},{1,0},{2,1},{3,2},{4,3},{5,4},{6,5},{7,6},{8,7},{9,8},{10,9... | collective-permute-start | bytes 786440 | tf_op jit(solution)/shard_map/ppermute | solution.py:29
  227.5 0.8 constant_dynamic-update-slice_fusion.4
  228.3 2.1 collective-permute-start.15
  231.9 0.8 constant_dynamic-update-slice_fusion.1
  232.7 6.1 %collective-permute-done.15 = bf16[1024,128]{1,0:T(8,128)(2,1)S(1)} collective-permute-done((bf16[1024,128]{1,0:T(8,128)(2,1)S(1)}, bf16[1024,128]{1,0:T(8,128)(2,1)S(1)}, u32[]{:S(2)}, u32[]{:S(2)}) %collective-permute-start.15) | collective-permute-done | bytes 262176 | tf_op jit(solution)/shard_map/ppermute | solution.py:24
  239.5 4.2 %convolution_convert_fusion = bf16[1024,128]{1,0:T(8,128)(2,1)} fusion(bf16[1024,2048]{1,0:T(8,128)(2,1)} %constant_dynamic-update-slice_fusion, bf16[1,2048,128]{2,1,0:T(8,128)(2,1)S(1)} %copy-done.16), kind=kOutput, calls=%fused_computation.15 | convolution fusion | flops 537001984 | bytes 4980736 | tf_op jit(solution)/shard_map/dot_general | solution.py:183
  243.6 16.9 %all-to-all-start.2 = ((bf16[32,32,128]{2,1,0:T(8,128)(2,1)}), bf16[32,32,128]{2,1,0:T(8,128)(2,1)S(1)}, u32[]{:S(2)}, u32[]{:S(2)}) async-start(bf16[32,32,128]{2,1,0:T(8,128)(2,1)} %bitcast.17), calls=%async_computation.2 | async-start | bytes 524288 | tf_op jit(solution)/shard_map/all_to_all | solution.py:185
  260.8 2.2 fusion.37
  263.0 19.8 %all-to-all-done.2 = bf16[32,32,128]{2,1,0:T(8,128)(2,1)S(1)} async-done(((bf16[32,32,128]{2,1,0:T(8,128)(2,1)}), bf16[32,32,128]{2,1,0:T(8,128)(2,1)S(1)}, u32[]{:S(2)}, u32[]{:S(2)}) %all-to-all-start.2) | async-done | bytes 262176 | tf_op jit(solution)/shard_map/all_to_all | solution.py:185
  282.8 1.3 gather_fusion.1
  284.2 1.1 fusion.24
  (246 shorter events, 13.0 us)
Async XLA Ops:
  7.2 122.0 %copy-start = (bf16[1,2048,128]{2,1,0:T(8,128)(2,1)S(1)}, bf16[1,2048,128]{2,1,0:T(8,128)(2,1)}, u32[]{:S(2)}) copy-start(bf16[1,2048,128]{2,1,0:T(8,128)(2,1)} %param.30) | copy-start | bytes 1572868
  7.2 117.8 %all-gather.2.cloned.1.call-start = ((), (), s32[]{:S(2)}) async-start(), calls=%async_computation.3 | async-start | bytes 4456448 | tf_op jit(solution)/shard_map/all_gather | solution.py:175
  16.7 46.1 %copy-start.3 = (bf16[256,2048]{1,0:T(8,128)(2,1)S(1)}, bf16[256,2048]{1,0:T(8,128)(2,1)}, u32[]{:S(2)}) copy-start(bf16[256,2048]{1,0:T(8,128)(2,1)} %param.16) | copy-start | bytes 3145732
  16.7 46.4 %copy-start.20 = (f32[2048]{0:T(1024)S(1)}, f32[2048]{0:T(1024)}, u32[]{:S(2)}) copy-start(f32[2048]{0:T(1024)} %param.17) | copy-start | bytes 24580
  22.7 44.3 %copy-start.14 = (f32[256,2]{0,1:T(2,128)S(1)}, f32[256,2]{0,1:T(2,128)}, u32[]{:S(2)}) copy-start(f32[256,2]{0,1:T(2,128)} %param.28) | copy-start | bytes 6148
  22.7 44.3 %copy-start.15 = (f32[4,128]{1,0:T(4,128)S(1)}, f32[4,128]{1,0:T(4,128)}, u32[]{:S(2)}) copy-start(f32[4,128]{1,0:T(4,128)} %param.20) | copy-start | bytes 6148
  22.7 44.4 %copy-start.21 = (f32[128]{0:T(128)S(1)}, f32[128]{0:T(128)}, u32[]{:S(2)}) copy-start(f32[128]{0:T(128)} %param.23) | copy-start | bytes 1540
  22.7 45.2 %copy-start.17 = (f32[256,128]{1,0:T(8,128)S(1)}, f32[256,128]{1,0:T(8,128)}, u32[]{:S(2)}) copy-start(f32[256,128]{1,0:T(8,128)} %param.24) | copy-start | bytes 393220
  22.8 45.2 %copy-start.18 = (bf16[1,128,128]{2,1,0:T(8,128)(2,1)S(1)}, bf16[1,128,128]{2,1,0:T(8,128)(2,1)}, u32[]{:S(2)}) copy-start(bf16[1,128,128]{2,1,0:T(8,128)(2,1)} %param.21) | copy-start | bytes 98308
  22.8 45.4 %copy-start.19 = (bf16[1,128,128]{2,1,0:T(8,128)(2,1)S(1)}, bf16[1,128,128]{2,1,0:T(8,128)(2,1)}, u32[]{:S(2)}) copy-start(bf16[1,128,128]{2,1,0:T(8,128)(2,1)} %param.22) | copy-start | bytes 98308
  64.6 60.4 %copy-start.4 = (bf16[1,2048,128]{2,1,0:T(8,128)(2,1)S(1)}, bf16[1,2048,128]{2,1,0:T(8,128)(2,1)}, u32[]{:S(2)}) copy-start(bf16[1,2048,128]{2,1,0:T(8,128)(2,1)} %param.29) | copy-start | bytes 1572868
  64.7 3.2 %collective-permute-start = (bf16[3,128]{1,0:T(4,128)(2,1)S(1)}, bf16[3,128]{1,0:T(4,128)(2,1)S(1)}, u32[]{:S(2)}, u32[]{:S(2)}) collective-permute-start(bf16[3,128]{1,0:T(4,128)(2,1)S(1)} %slice.443), channel_id=1, source_target_pairs={{0,16},{16,32},{32,48},{48,64},{64,80},{80,96},{96,112},{112,128},... | collective-permute-start | bytes 2312 | tf_op jit(solution)/shard_map/ppermute | solution.py:42
  68.4 60.2 %copy-start.5 = (f32[256,128]{1,0:T(8,128)}, f32[256,128]{1,0:T(8,128)S(1)}, u32[]{:S(2)}) copy-start(f32[256,128]{1,0:T(8,128)S(1)} %fusion.16) | copy-start | bytes 393220
  70.0 59.1 %copy-start.6 = (f32[256,128]{1,0:T(8,128)}, f32[256,128]{1,0:T(8,128)S(1)}, u32[]{:S(2)}) copy-start(f32[256,128]{1,0:T(8,128)S(1)} %pad.130) | copy-start | bytes 393220
  70.2 59.0 %copy-start.8 = (f32[256,128]{1,0:T(8,128)}, f32[256,128]{1,0:T(8,128)S(1)}, u32[]{:S(2)}) copy-start(f32[256,128]{1,0:T(8,128)S(1)} %pad.129) | copy-start | bytes 393220
  125.0 4.1 %copy-start.1 = (bf16[32,32,2048]{2,1,0:T(8,128)(2,1)S(1)}, bf16[32,32,2048]{2,1,0:T(8,128)(2,1)}, u32[]{:S(2)}) copy-start(bf16[32,32,2048]{2,1,0:T(8,128)(2,1)} %all-gather.2.cloned.1.call-done) | copy-start | bytes 12582916
  129.2 6.1 %slice-start = ((f32[256,128]{1,0:T(8,128)}), f32[1,128]{1,0:T(1,128)S(1)}, s32[]{:S(2)}) async-start(f32[256,128]{1,0:T(8,128)} %copy-done.5), calls=%async_computation.4 | async-start | bytes 1024 | tf_op jit(solution)/shard_map/slice | solution.py:148
  130.5 2.0 copy-start.2
  132.5 11.0 %collective-permute-start.1 = (bf16[1024,128]{1,0:T(8,128)(2,1)S(1)}, bf16[1024,128]{1,0:T(8,128)(2,1)S(1)}, u32[]{:S(2)}, u32[]{:S(2)}) collective-permute-start(bf16[1024,128]{1,0:T(8,128)(2,1)S(1)} %get-tuple-element.55), channel_id=1, source_target_pairs={{0,1},{1,2},{2,3},{3,4},{4,5},{5,6},{6,7},{7,8},{8,9},{9,10},{10,1... | collective-permute-start | bytes 786440 | tf_op jit(solution)/shard_map/ppermute | solution.py:24
  135.4 0.7 copy-start.10
  136.0 5.8 %copy-start.12 = (f32[256,128]{1,0:T(8,128)}, f32[256,128]{1,0:T(8,128)S(1)}, u32[]{:S(2)}) copy-start(f32[256,128]{1,0:T(8,128)S(1)} %pad.113) | copy-start | bytes 393220
  136.1 25.8 %collective-permute-start.2 = (bf16[1024,128]{1,0:T(8,128)(2,1)S(1)}, bf16[1024,128]{1,0:T(8,128)(2,1)S(1)}, u32[]{:S(2)}, u32[]{:S(2)}) collective-permute-start(bf16[1024,128]{1,0:T(8,128)(2,1)S(1)} %get-tuple-element.55), channel_id=1, source_target_pairs={{0,15},{1,0},{2,1},{3,2},{4,3},{5,4},{6,5},{7,6},{8,7},{9,8},{10,9... | collective-permute-start | bytes 786440 | tf_op jit(solution)/shard_map/ppermute | solution.py:29
  143.5 25.3 %collective-permute-start.3 = (bf16[1024,128]{1,0:T(8,128)(2,1)S(1)}, bf16[1024,128]{1,0:T(8,128)(2,1)S(1)}, u32[]{:S(2)}, u32[]{:S(2)}) collective-permute-start(bf16[1024,128]{1,0:T(8,128)(2,1)S(1)} %collective-permute-done.1), channel_id=1, source_target_pairs={{0,1},{1,2},{2,3},{3,4},{4,5},{5,6},{6,7},{7,8},{8,9},{9,10},{10,1... | collective-permute-start | bytes 786440 | tf_op jit(solution)/shard_map/ppermute | solution.py:24
  146.1 27.4 %all-to-all-start = ((f32[32,2,128]{2,1,0:T(2,128)}), f32[32,2,128]{2,1,0:T(2,128)S(1)}, u32[]{:S(2)}, u32[]{:S(2)}) async-start(f32[32,2,128]{2,1,0:T(2,128)} %broadcast_in_dim.50), calls=%async_computation | async-start | bytes 65536 | tf_op jit(solution)/shard_map/all_to_all | solution.py:47
  161.9 12.4 %collective-permute-start.4 = (bf16[1024,128]{1,0:T(8,128)(2,1)S(1)}, bf16[1024,128]{1,0:T(8,128)(2,1)S(1)}, u32[]{:S(2)}, u32[]{:S(2)}) collective-permute-start(bf16[1024,128]{1,0:T(8,128)(2,1)S(1)} %collective-permute-done.2), channel_id=1, source_target_pairs={{0,15},{1,0},{2,1},{3,2},{4,3},{5,4},{6,5},{7,6},{8,7},{9,8},{10,9... | collective-permute-start | bytes 786440 | tf_op jit(solution)/shard_map/ppermute | solution.py:29
  168.9 12.8 %collective-permute-start.5 = (bf16[1024,128]{1,0:T(8,128)(2,1)S(1)}, bf16[1024,128]{1,0:T(8,128)(2,1)S(1)}, u32[]{:S(2)}, u32[]{:S(2)}) collective-permute-start(bf16[1024,128]{1,0:T(8,128)(2,1)S(1)} %collective-permute-done.3), channel_id=1, source_target_pairs={{0,1},{1,2},{2,3},{3,4},{4,5},{5,6},{6,7},{7,8},{8,9},{9,10},{10,1... | collective-permute-start | bytes 786440 | tf_op jit(solution)/shard_map/ppermute | solution.py:24
  174.3 12.0 %collective-permute-start.6 = (bf16[1024,128]{1,0:T(8,128)(2,1)S(1)}, bf16[1024,128]{1,0:T(8,128)(2,1)S(1)}, u32[]{:S(2)}, u32[]{:S(2)}) collective-permute-start(bf16[1024,128]{1,0:T(8,128)(2,1)S(1)} %collective-permute-done.4), channel_id=1, source_target_pairs={{0,15},{1,0},{2,1},{3,2},{4,3},{5,4},{6,5},{7,6},{8,7},{9,8},{10,9... | collective-permute-start | bytes 786440 | tf_op jit(solution)/shard_map/ppermute | solution.py:29
  181.7 12.7 %collective-permute-start.7 = (bf16[1024,128]{1,0:T(8,128)(2,1)S(1)}, bf16[1024,128]{1,0:T(8,128)(2,1)}, u32[]{:S(2)}, u32[]{:S(2)}) collective-permute-start(bf16[1024,128]{1,0:T(8,128)(2,1)S(1)} %collective-permute-done.5), channel_id=1, source_target_pairs={{0,1},{1,2},{2,3},{3,4},{4,5},{5,6},{6,7},{7,8},{8,9},{9,10},{10,1... | collective-permute-start | bytes 786440 | tf_op jit(solution)/shard_map/ppermute | solution.py:24
  183.7 55.8 %copy-start.16 = (bf16[1,2048,128]{2,1,0:T(8,128)(2,1)S(1)}, bf16[1,2048,128]{2,1,0:T(8,128)(2,1)}, u32[]{:S(2)}) copy-start(bf16[1,2048,128]{2,1,0:T(8,128)(2,1)} %param.31) | copy-start | bytes 1572868
  186.2 11.6 %collective-permute-start.8 = (bf16[1024,128]{1,0:T(8,128)(2,1)S(1)}, bf16[1024,128]{1,0:T(8,128)(2,1)S(1)}, u32[]{:S(2)}, u32[]{:S(2)}) collective-permute-start(bf16[1024,128]{1,0:T(8,128)(2,1)S(1)} %collective-permute-done.6), channel_id=1, source_target_pairs={{0,15},{1,0},{2,1},{3,2},{4,3},{5,4},{6,5},{7,6},{8,7},{9,8},{10,9... | collective-permute-start | bytes 786440 | tf_op jit(solution)/shard_map/ppermute | solution.py:29
  194.4 11.1 %collective-permute-start.9 = (bf16[1024,128]{1,0:T(8,128)(2,1)}, bf16[1024,128]{1,0:T(8,128)(2,1)S(1)}, u32[]{:S(2)}, u32[]{:S(2)}) collective-permute-start(bf16[1024,128]{1,0:T(8,128)(2,1)} %collective-permute-done.7), channel_id=1, source_target_pairs={{0,1},{1,2},{2,3},{3,4},{4,5},{5,6},{6,7},{7,8},{8,9},{9,10},{10,1... | collective-permute-start | bytes 786440 | tf_op jit(solution)/shard_map/ppermute | solution.py:24
  197.9 12.1 %collective-permute-start.10 = (bf16[1024,128]{1,0:T(8,128)(2,1)S(1)}, bf16[1024,128]{1,0:T(8,128)(2,1)S(1)}, u32[]{:S(2)}, u32[]{:S(2)}) collective-permute-start(bf16[1024,128]{1,0:T(8,128)(2,1)S(1)} %collective-permute-done.8), channel_id=1, source_target_pairs={{0,15},{1,0},{2,1},{3,2},{4,3},{5,4},{6,5},{7,6},{8,7},{9,8},{10,9... | collective-permute-start | bytes 786440 | tf_op jit(solution)/shard_map/ppermute | solution.py:29
  205.6 11.8 %collective-permute-start.11 = (bf16[1024,128]{1,0:T(8,128)(2,1)S(1)}, bf16[1024,128]{1,0:T(8,128)(2,1)S(1)}, u32[]{:S(2)}, u32[]{:S(2)}) collective-permute-start(bf16[1024,128]{1,0:T(8,128)(2,1)S(1)} %collective-permute-done.9), channel_id=1, source_target_pairs={{0,1},{1,2},{2,3},{3,4},{4,5},{5,6},{6,7},{7,8},{8,9},{9,10},{10,1... | collective-permute-start | bytes 786440 | tf_op jit(solution)/shard_map/ppermute | solution.py:24
  209.9 10.9 %collective-permute-start.12 = (bf16[1024,128]{1,0:T(8,128)(2,1)S(1)}, bf16[1024,128]{1,0:T(8,128)(2,1)S(1)}, u32[]{:S(2)}, u32[]{:S(2)}) collective-permute-start(bf16[1024,128]{1,0:T(8,128)(2,1)S(1)} %collective-permute-done.10), channel_id=1, source_target_pairs={{0,15},{1,0},{2,1},{3,2},{4,3},{5,4},{6,5},{7,6},{8,7},{9,8},{10,9... | collective-permute-start | bytes 786440 | tf_op jit(solution)/shard_map/ppermute | solution.py:29
  217.4 10.9 %collective-permute-start.13 = (bf16[1024,128]{1,0:T(8,128)(2,1)S(1)}, bf16[1024,128]{1,0:T(8,128)(2,1)S(1)}, u32[]{:S(2)}, u32[]{:S(2)}) collective-permute-start(bf16[1024,128]{1,0:T(8,128)(2,1)S(1)} %collective-permute-done.11), channel_id=1, source_target_pairs={{0,1},{1,2},{2,3},{3,4},{4,5},{5,6},{6,7},{7,8},{8,9},{9,10},{10,1... | collective-permute-start | bytes 786440 | tf_op jit(solution)/shard_map/ppermute | solution.py:24
  220.8 11.1 %collective-permute-start.14 = (bf16[1024,128]{1,0:T(8,128)(2,1)S(1)}, bf16[1024,128]{1,0:T(8,128)(2,1)S(1)}, u32[]{:S(2)}, u32[]{:S(2)}) collective-permute-start(bf16[1024,128]{1,0:T(8,128)(2,1)S(1)} %collective-permute-done.12), channel_id=1, source_target_pairs={{0,15},{1,0},{2,1},{3,2},{4,3},{5,4},{6,5},{7,6},{8,7},{9,8},{10,9... | collective-permute-start | bytes 786440 | tf_op jit(solution)/shard_map/ppermute | solution.py:29
  228.3 10.4 %collective-permute-start.15 = (bf16[1024,128]{1,0:T(8,128)(2,1)S(1)}, bf16[1024,128]{1,0:T(8,128)(2,1)S(1)}, u32[]{:S(2)}, u32[]{:S(2)}) collective-permute-start(bf16[1024,128]{1,0:T(8,128)(2,1)S(1)} %collective-permute-done.13), channel_id=1, source_target_pairs={{0,1},{1,2},{2,3},{3,4},{4,5},{5,6},{6,7},{7,8},{8,9},{9,10},{10,1... | collective-permute-start | bytes 786440 | tf_op jit(solution)/shard_map/ppermute | solution.py:24
  231.2 29.6 %copy-start.7 = (f32[256,128]{1,0:T(8,128)S(1)}, f32[256,128]{1,0:T(8,128)}, u32[]{:S(2)}) copy-start(f32[256,128]{1,0:T(8,128)} %copy-done.6) | copy-start | bytes 393220
  231.2 29.6 %copy-start.9 = (f32[256,128]{1,0:T(8,128)S(1)}, f32[256,128]{1,0:T(8,128)}, u32[]{:S(2)}) copy-start(f32[256,128]{1,0:T(8,128)} %copy-done.8) | copy-start | bytes 393220
  231.2 29.6 %copy-start.11 = (f32[256,128]{1,0:T(8,128)S(1)}, f32[256,128]{1,0:T(8,128)}, u32[]{:S(2)}) copy-start(f32[256,128]{1,0:T(8,128)} %copy-done.10) | copy-start | bytes 393220
  231.2 29.7 %copy-start.13 = (f32[256,128]{1,0:T(8,128)S(1)}, f32[256,128]{1,0:T(8,128)}, u32[]{:S(2)}) copy-start(f32[256,128]{1,0:T(8,128)} %copy-done.12) | copy-start | bytes 393220
  243.6 39.2 %all-to-all-start.2 = ((bf16[32,32,128]{2,1,0:T(8,128)(2,1)}), bf16[32,32,128]{2,1,0:T(8,128)(2,1)S(1)}, u32[]{:S(2)}, u32[]{:S(2)}) async-start(bf16[32,32,128]{2,1,0:T(8,128)(2,1)} %bitcast.17), calls=%async_computation.2 | async-start | bytes 524288 | tf_op jit(solution)/shard_map/all_to_all | solution.py:185
Sparse Core Ops, SparseCore 0:
  62.9 62.0 all-gather.1
